TPU v7x, 32 devices: a whole 2x2x4 slice. The times are simulated.
32 devices in a mesh: sp: 8 (over z, x), tp: 4 (over y, core).
Axes of the slice: x: 2, y: 2, z: 4, core: 2. Of those that a mesh axis runs over, the one named last changes fastest.
Arguments:
- tokens: bfloat16 [2048, 2048], P('sp', 'tp'), may hold values from -6 to 6
- norm_gain: float32 [2048], replicated, may hold values from 0.1 to 1.9
- query_one: bfloat16 [2048, 512], P('sp', 'tp'), may hold values from -1 to 1
- key_one: bfloat16 [2048, 512], P('sp', 'tp'), may hold values from -1 to 1
- query_two: bfloat16 [2048, 512], P('sp', 'tp'), may hold values from -0.15625 to 0.15625
- key_two: bfloat16 [2048, 512], P('sp', 'tp'), may hold values from -0.15625 to 0.15625
- value_weight: bfloat16 [2048, 1024], P('sp', 'tp'), may hold values from -0.5 to 0.5
- pool_weight: bfloat16 [2048, 1024], P('sp', 'tp'), may hold values from -0.125 to 0.125
- lambda_head: float32 [8], replicated, may hold values from 0.3 to 0.8
- head_gain: float32 [128], replicated, may hold values from 0.1 to 1.9
- group_weight: bfloat16 [8, 128, 128], replicated, may hold values from -0.5 to 0.5
- pool_scale: float32 [1024], replicated, may hold values from 0.1 to 1.9
- out_attn: bfloat16 [1024, 2048], P('tp', 'sp'), may hold values from -0.125 to 0.125
- out_pool: bfloat16 [1024, 2048], P('tp', 'sp'), may hold values from -0.125 to 0.125
Outputs:
- mixed: bfloat16 [2048, 2048], P(('sp', 'tp'))
All inputs are finite; a program needn't handle non-finite values.
Results may differ from a plain program's by a relative error of at most 0.013.
Values may be sent and summed in bfloat16 or wider, within the bound.
A program may use at most 128 MiB of HBM per device.

v0:
```python
import math
import jax
import jax.numpy as jnp
from jax import lax
from jax.sharding import PartitionSpec as P

HEAD_DIM = 64
VALUE_DIM = 128
GROUP_DIM = 128
rope_base = 500000.0
head_scale = 0.8
norm_floor = 1e-06
head_floor = 0.001
masked_score = -1e30
pool_reach = 15
key_block = 1024


def from_behind(x, axis, by):
    peers = lax.axis_size(axis)
    pairs = [(i, i + by) for i in range(peers) if 0 <= i + by < peers]
    return lax.ppermute(x, axis, pairs)


def rotate(values_in, positions):
    half_dim = values_in.shape[-1] // 2
    inverse = rope_base ** (-(jnp.arange(half_dim, dtype=jnp.float32) * 2.0 / values_in.shape[-1]))
    angles = positions.astype(jnp.float32)[:, None] * inverse[None, :]
    cosine = jnp.cos(angles)[:, None, :]
    sine_part = jnp.sin(angles)[:, None, :]
    first_half = values_in[..., :half_dim]
    second_half = values_in[..., half_dim:]
    return jnp.concatenate(
        [
            first_half * cosine - second_half * sine_part,
            second_half * cosine + first_half * sine_part,
        ],
        axis=-1,
    )


def body(
    tokens,
    norm_gain,
    query_one,
    key_one,
    query_two,
    key_two,
    value_weight,
    pool_weight,
    lambda_head,
    head_gain,
    group_weight,
    pool_scale,
    out_attn,
    out_pool,
):
    tok_rows = tokens.shape[0]
    local_heads = query_one.shape[1] // HEAD_DIM
    local_groups = pool_weight.shape[1] // GROUP_DIM
    tp_index = lax.axis_index("tp")
    positions = lax.axis_index("sp") * tok_rows + jnp.arange(tok_rows, dtype=jnp.int32)
    score_scale = HEAD_DIM ** (-0.5)
    gathered = lax.all_gather(tokens, "tp", axis=1, tiled=True)
    float_rows = gathered.astype(jnp.float32)
    normed = (
        float_rows
        * lax.rsqrt(jnp.mean(float_rows * float_rows, axis=-1, keepdims=True) + norm_floor)
        * norm_gain
    ).astype(jnp.bfloat16)

    def contract(shard_part):
        return jnp.dot(normed, shard_part, preferred_element_type=jnp.float32)

    pieces = (
        lax.all_gather(query_one, "sp", axis=0, tiled=True),
        lax.all_gather(key_one, "sp", axis=0, tiled=True),
        lax.all_gather(query_two, "sp", axis=0, tiled=True),
        lax.all_gather(key_two, "sp", axis=0, tiled=True),
        lax.all_gather(value_weight, "sp", axis=0, tiled=True),
    )
    projected = tuple((contract(shard_part) for shard_part in pieces))
    pool_proj = contract(lax.all_gather(pool_weight, "sp", axis=0, tiled=True))

    def turned(flat_part):
        return rotate(flat_part.reshape(tok_rows, local_heads, HEAD_DIM), positions).astype(
            jnp.bfloat16
        )

    query_a = turned(projected[0])
    key_a = turned(projected[1]).reshape(tok_rows, local_heads * HEAD_DIM)
    query_b = turned(projected[2])
    key_b = turned(projected[3]).reshape(tok_rows, local_heads * HEAD_DIM)
    value_rows = projected[4].astype(jnp.bfloat16)
    queries = (query_a, query_b)
    initial = (
        jnp.full((2, tok_rows, local_heads), masked_score, jnp.float32),
        jnp.zeros((2, tok_rows, local_heads), jnp.float32),
        jnp.zeros((2, tok_rows, local_heads, VALUE_DIM), jnp.float32),
    )
    pieces = (
        lax.all_gather(key_a, "sp", axis=0, tiled=True),
        lax.all_gather(key_b, "sp", axis=0, tiled=True),
        lax.all_gather(value_rows, "sp", axis=0, tiled=True),
    )
    key_rows = pieces[0].shape[0]
    key_span = math.gcd(key_rows, key_block)
    count_blocks = key_rows // key_span
    stacked = tuple((member.reshape(count_blocks, key_span, local_heads, -1) for member in pieces))

    def step_block(carried, inputs):
        maxima, totals, accums = carried
        block_a, block_b, block_v, block_id = inputs
        key_pos = block_id * key_span + jnp.arange(key_span, dtype=jnp.int32)
        visible = (key_pos[None, :] <= positions[:, None])[:, None, :]
        new_maxima, new_totals, new_accums = ([], [], [])
        for map_index, key_part in enumerate((block_a, block_b)):
            scores = (
                jnp.einsum(
                    "qhd,khd->qhk", queries[map_index], key_part, preferred_element_type=jnp.float32
                )
                * score_scale
            )
            scores = jnp.where(visible, scores, masked_score)
            top_now = jnp.maximum(maxima[map_index], jnp.max(scores, axis=-1))
            factor = jnp.exp(maxima[map_index] - top_now)
            weights = jnp.where(visible, jnp.exp(scores - top_now[..., None]), 0.0)
            new_maxima.append(top_now)
            new_totals.append(totals[map_index] * factor + jnp.sum(weights, axis=-1))
            product = jnp.einsum(
                "qhk,khd->qhd",
                weights.astype(jnp.bfloat16),
                block_v,
                preferred_element_type=jnp.float32,
            )
            new_accums.append(accums[map_index] * factor[..., None] + product)
        return ((jnp.stack(new_maxima), jnp.stack(new_totals), jnp.stack(new_accums)), None)

    result_state, _ = lax.scan(
        step_block,
        initial,
        (stacked[0], stacked[1], stacked[2], jnp.arange(count_blocks, dtype=jnp.int32)),
    )
    maxima, totals, accums = result_state
    map_means = accums / totals[..., None]
    lambda_local = lax.dynamic_slice_in_dim(lambda_head, tp_index * local_heads, local_heads, 0)
    differed = map_means[0] - lambda_local[None, :, None] * map_means[1]
    scaled = (
        differed
        * lax.rsqrt(jnp.mean(differed * differed, axis=-1, keepdims=True) + head_floor)
        * head_gain
        * head_scale
    )
    attn_out = scaled.reshape(tok_rows, local_heads * VALUE_DIM).astype(jnp.bfloat16)
    pool_rows = pool_proj.astype(jnp.bfloat16)
    prior_rows = from_behind(pool_rows[tok_rows - pool_reach :], "sp", 1)
    extended = jnp.concatenate([prior_rows, pool_rows], axis=0).astype(jnp.float32)
    group_ids = tp_index * local_groups + jnp.arange(local_groups, dtype=jnp.int32)
    windows = jnp.left_shift(2, group_ids % 4)
    channel_windows = (windows[:, None] + jnp.zeros((1, GROUP_DIM), jnp.int32)).reshape(-1)
    window_sum = jnp.zeros((tok_rows, local_groups * GROUP_DIM), jnp.float32)
    for lag_steps in range(pool_reach + 1):
        keep_mask = (lag_steps < channel_windows).astype(jnp.float32)
        window_sum = (
            window_sum
            + extended[pool_reach - lag_steps : pool_reach - lag_steps + tok_rows]
            * keep_mask[None, :]
        )
    counts = jnp.minimum(positions[:, None] + 1, channel_windows[None, :]).astype(jnp.float32)
    window_mean = window_sum / counts - pool_rows.astype(jnp.float32)
    local_mixing = lax.dynamic_slice_in_dim(group_weight, tp_index * local_groups, local_groups, 0)
    grouped = jnp.einsum(
        "tgc,gcd->tgd",
        window_mean.astype(jnp.bfloat16).reshape(tok_rows, local_groups, GROUP_DIM),
        local_mixing,
        preferred_element_type=jnp.float32,
    )
    scale_local = lax.dynamic_slice_in_dim(
        pool_scale, tp_index * local_groups * GROUP_DIM, local_groups * GROUP_DIM, 0
    )
    pooled = (grouped.reshape(tok_rows, local_groups * GROUP_DIM) * scale_local).astype(
        jnp.bfloat16
    )
    attn_cols, pool_cols = (
        lax.all_gather(out_attn, "sp", axis=1, tiled=True),
        lax.all_gather(out_pool, "sp", axis=1, tiled=True),
    )
    return lax.psum_scatter(
        (
            jnp.dot(attn_out, attn_cols, preferred_element_type=jnp.float32)
            + jnp.dot(pooled, pool_cols, preferred_element_type=jnp.float32)
        ).astype(jnp.bfloat16),
        "tp",
        scatter_dimension=0,
        tiled=True,
    )


def solution(mesh):
    in_specs = (
        P("sp", "tp"),
        P(),
        P("sp", "tp"),
        P("sp", "tp"),
        P("sp", "tp"),
        P("sp", "tp"),
        P("sp", "tp"),
        P("sp", "tp"),
        P(),
        P(),
        P(),
        P(),
        P("tp", "sp"),
        P("tp", "sp"),
    )
    out_specs = P(("sp", "tp"), None)
    return jax.shard_map(body, mesh=mesh, in_specs=in_specs, out_specs=out_specs, check_vma=False)
```

profile of v0, /device:TPU:0, one launch (start us, length us, event | category | flops | bytes accessed | tf_op | source)
XLA Modules:
  0.0 335.7 jit_solution(8059476277659263844)
XLA Ops:
  6.5 0.7 all-gather.7.cloned.1.call-update
  7.3 0.7 all-gather.9.cloned.1.call-update
  8.1 0.7 all-gather.15.cloned.1.call-update
  8.8 19.6 %all-gather.7.cloned.1.call-done = bf16[256,2048]{1,0:T(8,128)(2,1)} async-done(((bf16[256,512]{1,0:T(8,128)(2,1)}), bf16[256,2048]{1,0:T(8,128)(2,1)}) %all-gather.7.cloned.1.call-update) | async-done | bytes 1048592 | tf_op jit(solution)/shard_map/all_gather | solution.py:64
  28.4 1.5 fusion.41
  29.9 1.6 fusion.43
  31.5 39.3 %all-gather.9.cloned.1.call-done = bf16[2048,256]{1,0:T(8,128)(2,1)} async-done(((bf16[256,256]{1,0:T(8,128)(2,1)}), bf16[2048,256]{1,0:T(8,128)(2,1)}) %all-gather.9.cloned.1.call-update) | async-done | bytes 1048592 | tf_op jit(solution)/shard_map/all_gather | solution.py:80
  70.8 2.3 convolution_convert_fusion.1
  73.1 0.0 all-gather.13.cloned.1.call-start
  73.2 0.5 all-gather.13.cloned.1.call-update
  73.8 0.5 all-gather.17.cloned.1.call-update
  74.4 0.1 fusion.75
  74.5 0.6 broadcast_bitcast_fusion.1
  75.1 0.5 fusion.91
  75.6 31.9 %all_gather.37 = bf16[2048,128]{1,0:T(8,128)(2,1)S(1)} all-gather(bf16[256,128]{1,0:T(8,128)(2,1)S(1)} %copy-done.4), channel_id=1, replica_groups=mesh['sp'=8,'tp'=4] {'sp'}, dimensions={0}, use_global_device_ids=true | all-gather | bytes 589824 | tf_op jit(solution)/shard_map/all_gather | solution.py:77
  107.5 32.2 %all_gather.39 = bf16[2048,128]{1,0:T(8,128)(2,1)S(1)} all-gather(bf16[256,128]{1,0:T(8,128)(2,1)S(1)} %copy-done.5), channel_id=1, replica_groups=mesh['sp'=8,'tp'=4] {'sp'}, dimensions={0}, use_global_device_ids=true | all-gather | bytes 589824 | tf_op jit(solution)/shard_map/all_gather | solution.py:76
  139.7 32.3 %all_gather.40 = bf16[2048,128]{1,0:T(8,128)(2,1)S(1)} all-gather(bf16[256,128]{1,0:T(8,128)(2,1)S(1)} %copy-done.6), channel_id=1, replica_groups=mesh['sp'=8,'tp'=4] {'sp'}, dimensions={0}, use_global_device_ids=true | all-gather | bytes 589824 | tf_op jit(solution)/shard_map/all_gather | solution.py:79
  172.0 31.9 %all_gather.42 = bf16[2048,128]{1,0:T(8,128)(2,1)S(1)} all-gather(bf16[256,128]{1,0:T(8,128)(2,1)S(1)} %copy-done.7), channel_id=1, replica_groups=mesh['sp'=8,'tp'=4] {'sp'}, dimensions={0}, use_global_device_ids=true | all-gather | bytes 589824 | tf_op jit(solution)/shard_map/all_gather | solution.py:78
  203.9 0.2 multiply_cosine_fusion
  204.1 0.7 dynamic_slice.24
  204.9 0.1 broadcast_bitcast_fusion
  204.9 0.8 dynamic_slice.26
  205.7 0.5 fusion.97
  206.2 0.5 fusion.98
  206.7 0.5 fusion.99
  207.2 0.5 fusion.100
  207.7 0.1 subtract_convert_fusion
  207.8 32.2 %all_gather.41 = bf16[2048,128]{0,1:T(8,128)(2,1)S(1)} all-gather(bf16[256,128]{0,1:T(8,128)(2,1)S(1)} %bitcast.251), channel_id=1, replica_groups=mesh['sp'=8,'tp'=4] {'sp'}, dimensions={0}, use_global_device_ids=true | all-gather | bytes 589824 | tf_op jit(solution)/shard_map/all_gather | solution.py:103
  240.0 31.2 %all_gather.38 = bf16[2048,128]{0,1:T(8,128)(2,1)S(1)} all-gather(bf16[256,128]{0,1:T(8,128)(2,1)S(1)} %bitcast.252), channel_id=1, replica_groups=mesh['sp'=8,'tp'=4] {'sp'}, dimensions={0}, use_global_device_ids=true | all-gather | bytes 589824 | tf_op jit(solution)/shard_map/all_gather | solution.py:102
  271.1 1.7 convolution_convert_fusion
  272.8 1.5 collective-permute-start
  274.3 0.4 reshape.311
  274.7 0.9 copy.23
  275.6 0.4 reshape.308
  276.0 0.1 copy.22
  276.2 0.7 fusion.70
  277.0 0.1 fusion.61
  277.1 1.3 reshape.313
  278.5 18.7 %while.15 = (s32[]{:T(128)}, f32[2,256,2]{1,2,0:T(2,128)S(1)}, f32[2,256,2]{1,2,0:T(2,128)S(1)}, f32[2,256,2,128]{1,3,2,0:T(8,128)S(1)}, s32[2]{0:T(128)S(1)}, /...) while((s32[]{:T(128)}, f32[2,256,2]{1,2,0:T(2,128)S(1)}, ...), condition=%wide.region_6.7_spmd.clone, body=%wide.region_1.6_spmd.clone.sunk | while | flops 416947456 | bytes 34822424 | solution.py:139
  278.6 0.7 dynamic_slice.53
  279.9 0.2 broadcast_compare_fusion.2
  280.1 1.8 fusion.141
  282.0 0.4 constant_dynamic-slice_fusion.2
  282.4 0.4 copy.37
  282.8 2.4 fusion.147
  285.2 1.0 fusion.143
  286.2 0.6 fusion.146
  286.9 0.6 fusion.145
  287.5 0.4 copy-done.3
  287.9 0.7 dynamic_slice.53
  289.2 0.2 broadcast_compare_fusion.2
  289.5 1.8 fusion.141
  291.3 0.4 constant_dynamic-slice_fusion.2
  291.7 0.4 copy.37
  292.1 2.4 fusion.147
  294.5 1.0 fusion.143
  295.5 0.6 fusion.146
  296.2 0.6 fusion.145
  296.9 0.4 copy-done.3
  297.3 0.1 fusion.67
  297.5 0.1 fusion.64
  297.6 1.7 fusion.101
  299.4 2.7 fusion.40
  302.1 26.7 %reduce-scatter.2.cloned.1.call-done = bf16[64,2048]{1,0:T(8,128)(2,1)} async-done(((bf16[256,2048]{1,0:T(8,128)(2,1)}), bf16[64,2048]{1,0:T(8,128)(2,1)}) %reduce-scatter.2.cloned.1.call-update) | async-done | bytes 262160 | tf_op jit(solution)/shard_map/reduce_scatter | solution.py:188
  (73 shorter events, 0.8 us)
Async XLA Ops:
  6.5 269.7 %copy-start = (bf16[8,128,128]{2,1,0:T(8,128)(2,1)S(1)}, bf16[8,128,128]{2,1,0:T(8,128)(2,1)}, u32[]{:S(2)}) copy-start(bf16[8,128,128]{2,1,0:T(8,128)(2,1)} %param.26) | copy-start | bytes 786436
  6.5 21.8 %all-gather.7.cloned.1.call-start = ((), (), s32[]{:S(2)}) async-start(), calls=%async_computation.1 | async-start | bytes 1310720 | tf_op jit(solution)/shard_map/all_gather | solution.py:64
  7.3 63.5 %all-gather.9.cloned.1.call-start = ((), (), s32[]{:S(2)}) async-start(), calls=%async_computation.2 | async-start | bytes 1179648 | tf_op jit(solution)/shard_map/all_gather | solution.py:80
  8.0 263.1 %all-gather.15.cloned.1.call-start = ((), (), s32[]{:S(2)}) async-start(), calls=%async_computation.5 | async-start | bytes 1179648 | tf_op jit(solution)/shard_map/all_gather | solution.py:83
  8.7 268.4 %all-gather.11.cloned.1.call-start = ((), (), s32[]{:S(2)}) async-start(), calls=%async_computation.3 | async-start | bytes 1179648 | tf_op jit(solution)/shard_map/all_gather | solution.py:104
  29.9 45.7 %copy-start.4 = (bf16[256,128]{1,0:T(8,128)(2,1)S(1)}, bf16[256,128]{1,0:T(8,128)(2,1)}, u32[]{:S(2)}) copy-start(bf16[256,128]{1,0:T(8,128)(2,1)} %param.19) | copy-start | bytes 196612
  31.5 76.1 %copy-start.5 = (bf16[256,128]{1,0:T(8,128)(2,1)S(1)}, bf16[256,128]{1,0:T(8,128)(2,1)}, u32[]{:S(2)}) copy-start(bf16[256,128]{1,0:T(8,128)(2,1)} %param.18) | copy-start | bytes 196612
  31.5 108.2 %copy-start.6 = (bf16[256,128]{1,0:T(8,128)(2,1)S(1)}, bf16[256,128]{1,0:T(8,128)(2,1)}, u32[]{:S(2)}) copy-start(bf16[256,128]{1,0:T(8,128)(2,1)} %param.21) | copy-start | bytes 196612
  31.5 140.5 %copy-start.7 = (bf16[256,128]{1,0:T(8,128)(2,1)S(1)}, bf16[256,128]{1,0:T(8,128)(2,1)}, u32[]{:S(2)}) copy-start(bf16[256,128]{1,0:T(8,128)(2,1)} %param.20) | copy-start | bytes 196612
  31.5 173.4 %copy-start.8 = (f32[128]{0:T(128)S(1)}, f32[128]{0:T(128)}, u32[]{:S(2)}) copy-start(f32[128]{0:T(128)} %param.25) | copy-start | bytes 1540
  73.1 224.5 %all-gather.13.cloned.1.call-start = ((), (), s32[]{:S(2)}) async-start(), calls=%async_computation.4 | async-start | bytes 1179648 | tf_op jit(solution)/shard_map/all_gather | solution.py:185
  73.7 225.6 %all-gather.17.cloned.1.call-start = ((), (), s32[]{:S(2)}) async-start(), calls=%async_computation.6 | async-start | bytes 1179648 | tf_op jit(solution)/shard_map/all_gather | solution.py:186
  74.3 254.5 %reduce-scatter.2.cloned.1.call-start = ((), (), s32[]{:S(2)}) async-start(), calls=%async_computation.7 | async-start | bytes 1310720 | tf_op jit(solution)/shard_map/reduce_scatter | solution.py:188
  272.8 3.3 collective-permute-start
  274.3 1.9 copy-start.10
  274.3 1.9 copy-start.11
  278.5 3.4 %copy-start.2 = (bf16[2,1024,2,64]{1,3,2,0:T(8,128)(2,1)}, bf16[2,1024,2,64]{1,3,2,0:T(8,128)(2,1)S(1)}, u32[]{:S(2)}) copy-start(bf16[2,1024,2,64]{1,3,2,0:T(8,128)(2,1)S(1)} %get-tuple-element.317) | copy-start | bytes 1572868 | tf_op jit(solution)/shard_map/while
  282.8 2.4 copy-start.1
  282.8 2.4 copy-start.9
  286.9 1.0 copy-start.3
  287.9 3.4 %copy-start.2 = (bf16[2,1024,2,64]{1,3,2,0:T(8,128)(2,1)}, bf16[2,1024,2,64]{1,3,2,0:T(8,128)(2,1)S(1)}, u32[]{:S(2)}) copy-start(bf16[2,1024,2,64]{1,3,2,0:T(8,128)(2,1)S(1)} %get-tuple-element.317) | copy-start | bytes 1572868 | tf_op jit(solution)/shard_map/while
  292.1 2.4 copy-start.1
  292.1 2.4 copy-start.9
  296.2 1.0 copy-start.3
Sparse Core Ops, SparseCore 0:
  8.9 19.4 all-gather.6
  30.5 40.2 all-gather.8
  72.9 41.6 all-gather.14
  116.6 41.4 all-gather.10
  160.0 42.5 all-gather.12
  204.4 40.6 all-gather.16
  302.2 26.5 reduce-scatter.1
where the time goes:
time: 336 us
  blocking collectives  192 us (57%)
  waiting for transfers between devices  88.8 us (26%)
  matrix products  22.8 us (7%)
  between operations  13.8 us (4%)
  local copies, waits for them, and re-layouts  9.14 us (3%)
  other arithmetic  6.18 us (2%)
    all_gather x1, waiting for transfers between devices, body(): lax.all_gather(value_weight, 'sp', axis=0, tiled=True)  39.3 us
    all_gather x1, blocking collectives, body(): lax.all_gather(key_two, 'sp', axis=0, tiled=True)  32.3 us
    all_gather x1, blocking collectives, body(): lax.all_gather(key_b, 'sp', axis=0, tiled=True)  32.2 us
    all_gather x1, blocking collectives, body(): lax.all_gather(query_one, 'sp', axis=0, tiled=True)  32.2 us
    all_gather x1, blocking collectives, body(): lax.all_gather(query_two, 'sp', axis=0, tiled=True)  31.9 us
    all_gather x1, blocking collectives, body(): lax.all_gather(key_one, 'sp', axis=0, tiled=True)  31.9 us
    all_gather x1, blocking collectives, body(): lax.all_gather(key_a, 'sp', axis=0, tiled=True)  31.2 us
    reduce_scatter x1, waiting for transfers between devices, body(): lax.psum_scatter((jnp.dot(attn_out, attn_cols, preferred_element_type=jnp...  26.7 us
  transfers between devices with their start and end apart: 8, of which 3 were waited for; matrix products, arithmetic and copies ran while one was open for 10% of the time, Pallas kernels for 0%

commit v1 on v0

--- a/solution.py
+++ b/solution.py
@@ -61,7 +61,7 @@
     tp_index = lax.axis_index("tp")
     positions = lax.axis_index("sp") * tok_rows + jnp.arange(tok_rows, dtype=jnp.int32)
     score_scale = HEAD_DIM ** (-0.5)
-    gathered = lax.all_gather(tokens, "tp", axis=1, tiled=True)
+    gathered = jnp.concatenate(lax.all_gather(tokens, "tp"), axis=1)
     float_rows = gathered.astype(jnp.float32)
     normed = (
         float_rows

time: 336 us -> 342 us (1.018)
  local copies, waits for them, and re-layouts: 9.14 us -> 16.1 us
  waiting for transfers between devices: 88.8 us -> 82.9 us
    all_gather x1, waiting for transfers between devices: 39.3 us -> 34.3 us  [body(): lax.all_gather(value_weight, 'sp', axis=0, tiled=True)]
    dot_general x0 -> x4, local copies, waits for them, and re-layouts: none -> 4.05 us  [contract(): return jnp.dot(normed, shard_part, preferred_element_type=jnp.float32)]
  transfers between devices with their start and end apart: 8 -> 8, of which waited for: 3 -> 3; matrix products, arithmetic and copies ran while one was open for 10% -> 13% of each run, Pallas kernels for 0% -> 0%
where the time goes in v1:
time: 342 us; the launch traced here: 341 us
  blocking collectives  191 us (56%)
  waiting for transfers between devices  82.9 us (24%)
  matrix products  24.3 us (7%)
  local copies, waits for them, and re-layouts  16.1 us (5%)
  between operations  13.9 us (4%)
  other arithmetic  9.06 us (3%)
    all_gather x1, waiting for transfers between devices, body(): lax.all_gather(value_weight, 'sp', axis=0, tiled=True)  34.3 us
    all_gather x1, blocking collectives, body(): lax.all_gather(key_two, 'sp', axis=0, tiled=True)  32.4 us
    all_gather x1, blocking collectives, body(): lax.all_gather(key_b, 'sp', axis=0, tiled=True)  32.2 us
    all_gather x1, blocking collectives, body(): lax.all_gather(query_two, 'sp', axis=0, tiled=True)  32 us
    all_gather x1, blocking collectives, body(): lax.all_gather(query_one, 'sp', axis=0, tiled=True)  31.8 us
    all_gather x1, blocking collectives, body(): lax.all_gather(key_one, 'sp', axis=0, tiled=True)  31.7 us
    all_gather x1, blocking collectives, body(): lax.all_gather(key_a, 'sp', axis=0, tiled=True)  31.2 us
    reduce_scatter x1, waiting for transfers between devices, body(): lax.psum_scatter((jnp.dot(attn_out, attn_cols, preferred_element_type=jnp...  25.8 us
  transfers between devices with their start and end apart: 8, of which 3 were waited for; matrix products, arithmetic and copies ran while one was open for 13% of the time, Pallas kernels for 0%

profile of v1, /device:TPU:0, one launch (start us, length us, event | category | flops | bytes accessed | tf_op | source)
XLA Modules:
  0.0 340.9 jit_solution(18240347365860580711)
XLA Ops:
  6.5 0.7 all-gather.18.cloned.1.call-update
  7.3 0.7 all-gather.8.cloned.1.call-update
  8.1 0.7 all-gather.14.cloned.1.call-update
  8.8 19.6 %all-gather.18.cloned.1.call-done = bf16[1024,512]{1,0:T(8,128)(2,1)} async-done(((bf16[256,512]{1,0:T(8,128)(2,1)}), bf16[1024,512]{1,0:T(8,128)(2,1)}) %all-gather.18.cloned.1.call-update) | async-done | bytes 1048592 | tf_op jit(solution)/shard_map/all_gather | solution.py:64
  28.4 2.8 convert_bitcast_fusion
  31.2 3.0 copy.63
  34.2 0.3 fusion.41
  34.5 1.9 fusion.45
  36.5 34.3 %all-gather.8.cloned.1.call-done = bf16[2048,256]{1,0:T(8,128)(2,1)} async-done(((bf16[256,256]{1,0:T(8,128)(2,1)}), bf16[2048,256]{1,0:T(8,128)(2,1)}) %all-gather.8.cloned.1.call-update) | async-done | bytes 1048592 | tf_op jit(solution)/shard_map/all_gather | solution.py:80
  70.8 2.4 convolution_convert_fusion.1
  73.2 0.5 all-gather.12.cloned.1.call-update
  73.8 0.5 all-gather.16.cloned.1.call-update
  74.4 0.7 fusion.78
  75.1 0.6 broadcast_bitcast_fusion.1
  75.7 0.5 fusion.94
  76.3 31.7 %all_gather.41 = bf16[2048,128]{1,0:T(8,128)(2,1)S(1)} all-gather(bf16[256,128]{1,0:T(8,128)(2,1)S(1)} %copy-done.7), channel_id=1, replica_groups=mesh['sp'=8,'tp'=4] {'sp'}, dimensions={0}, use_global_device_ids=true | all-gather | bytes 589824 | tf_op jit(solution)/shard_map/all_gather | solution.py:77
  108.0 1.0 copy.55
  109.0 31.8 %all_gather.43 = bf16[2048,128]{1,0:T(8,128)(2,1)S(1)} all-gather(bf16[256,128]{1,0:T(8,128)(2,1)S(1)} %copy-done.8), channel_id=1, replica_groups=mesh['sp'=8,'tp'=4] {'sp'}, dimensions={0}, use_global_device_ids=true | all-gather | bytes 589824 | tf_op jit(solution)/shard_map/all_gather | solution.py:76
  140.8 1.0 copy.57
  141.8 32.4 %all_gather.44 = bf16[2048,128]{1,0:T(8,128)(2,1)S(1)} all-gather(bf16[256,128]{1,0:T(8,128)(2,1)S(1)} %copy-done.9), channel_id=1, replica_groups=mesh['sp'=8,'tp'=4] {'sp'}, dimensions={0}, use_global_device_ids=true | all-gather | bytes 589824 | tf_op jit(solution)/shard_map/all_gather | solution.py:79
  174.2 1.0 copy.59
  175.2 32.0 %all_gather.46 = bf16[2048,128]{1,0:T(8,128)(2,1)S(1)} all-gather(bf16[256,128]{1,0:T(8,128)(2,1)S(1)} %copy-done.10), channel_id=1, replica_groups=mesh['sp'=8,'tp'=4] {'sp'}, dimensions={0}, use_global_device_ids=true | all-gather | bytes 589824 | tf_op jit(solution)/shard_map/all_gather | solution.py:78
  207.3 1.0 copy.61
  208.3 0.2 multiply_cosine_fusion
  208.6 0.8 dynamic_slice.26
  209.4 0.3 fusion.46
  209.7 0.5 copy.54
  210.3 1.4 fusion.100
  211.7 1.4 fusion.101
  213.1 0.3 fusion.102
  213.4 0.3 fusion.103
  213.8 32.2 %all_gather.45 = bf16[2048,128]{0,1:T(8,128)(2,1)S(1)} all-gather(bf16[256,128]{0,1:T(8,128)(2,1)S(1)} %bitcast.284), channel_id=1, replica_groups=mesh['sp'=8,'tp'=4] {'sp'}, dimensions={0}, use_global_device_ids=true | all-gather | bytes 589824 | tf_op jit(solution)/shard_map/all_gather | solution.py:103
  246.0 31.2 %all_gather.42 = bf16[2048,128]{0,1:T(8,128)(2,1)S(1)} all-gather(bf16[256,128]{0,1:T(8,128)(2,1)S(1)} %bitcast.285), channel_id=1, replica_groups=mesh['sp'=8,'tp'=4] {'sp'}, dimensions={0}, use_global_device_ids=true | all-gather | bytes 589824 | tf_op jit(solution)/shard_map/all_gather | solution.py:102
  277.2 1.7 convolution_convert_fusion
  278.9 1.5 collective-permute-start
  280.5 0.4 reshape.349
  280.9 0.9 copy.65
  281.8 0.4 reshape.348
  282.4 0.7 fusion.73
  283.3 1.3 reshape.350
  284.7 18.7 %while.15 = (s32[]{:T(128)}, f32[2,256,2]{1,2,0:T(2,128)S(1)}, f32[2,256,2]{1,2,0:T(2,128)S(1)}, f32[2,256,2,128]{1,3,2,0:T(8,128)S(1)}, s32[2]{0:T(128)S(1)}, /...) while((s32[]{:T(128)}, f32[2,256,2]{1,2,0:T(2,128)S(1)}, ...), condition=%wide.region_6.7_spmd.clone, body=%wide.region_1.6_spmd.clone.sunk | while | flops 416947456 | bytes 34822424 | solution.py:139
  284.8 0.7 dynamic_slice.53
  286.1 0.2 broadcast_compare_fusion.2
  286.3 1.9 fusion.144
  288.2 0.4 constant_dynamic-slice_fusion.2
  288.6 0.4 copy.87
  289.0 2.4 fusion.150
  291.4 1.0 fusion.146
  292.4 0.6 fusion.149
  293.1 0.6 fusion.148
  293.7 0.4 copy-done.6
  294.1 0.7 dynamic_slice.53
  295.5 0.2 broadcast_compare_fusion.2
  295.7 1.9 fusion.144
  297.6 0.4 constant_dynamic-slice_fusion.2
  297.9 0.4 copy.87
  298.4 2.4 fusion.150
  300.8 1.0 fusion.146
  301.8 0.6 fusion.149
  302.5 0.6 fusion.148
  303.1 0.4 copy-done.6
  303.9 1.7 fusion.104
  305.6 2.7 fusion.40
  308.3 25.8 %reduce-scatter.2.cloned.1.call-done = bf16[64,2048]{1,0:T(8,128)(2,1)} async-done(((bf16[256,2048]{1,0:T(8,128)(2,1)}), bf16[64,2048]{1,0:T(8,128)(2,1)}) %reduce-scatter.2.cloned.1.call-update) | async-done | bytes 262160 | tf_op jit(solution)/shard_map/reduce_scatter | solution.py:188
  (98 shorter events, 1.5 us)
Async XLA Ops:
  6.5 275.8 %copy-start = (bf16[8,128,128]{2,1,0:T(8,128)(2,1)S(1)}, bf16[8,128,128]{2,1,0:T(8,128)(2,1)}, u32[]{:S(2)}) copy-start(bf16[8,128,128]{2,1,0:T(8,128)(2,1)} %param.26) | copy-start | bytes 786436
  6.5 21.8 %all-gather.18.cloned.1.call-start = ((), (), s32[]{:S(2)}) async-start(), calls=%async_computation.7 | async-start | bytes 1310720 | tf_op jit(solution)/shard_map/all_gather | solution.py:64
  7.3 63.5 %all-gather.8.cloned.1.call-start = ((), (), s32[]{:S(2)}) async-start(), calls=%async_computation.1 | async-start | bytes 1179648 | tf_op jit(solution)/shard_map/all_gather | solution.py:80
  8.0 269.2 %all-gather.14.cloned.1.call-start = ((), (), s32[]{:S(2)}) async-start(), calls=%async_computation.4 | async-start | bytes 1179648 | tf_op jit(solution)/shard_map/all_gather | solution.py:83
  8.7 274.6 %all-gather.10.cloned.1.call-start = ((), (), s32[]{:S(2)}) async-start(), calls=%async_computation.2 | async-start | bytes 1179648 | tf_op jit(solution)/shard_map/all_gather | solution.py:104
  31.2 3.0 copy-start.1
  31.2 3.3 copy-start.11
  36.4 39.8 %copy-start.7 = (bf16[256,128]{1,0:T(8,128)(2,1)S(1)}, bf16[256,128]{1,0:T(8,128)(2,1)}, u32[]{:S(2)}) copy-start(bf16[256,128]{1,0:T(8,128)(2,1)} %param.19) | copy-start | bytes 196612
  36.5 72.6 %copy-start.8 = (bf16[256,128]{1,0:T(8,128)(2,1)S(1)}, bf16[256,128]{1,0:T(8,128)(2,1)}, u32[]{:S(2)}) copy-start(bf16[256,128]{1,0:T(8,128)(2,1)} %param.18) | copy-start | bytes 196612
  73.1 68.7 %copy-start.9 = (bf16[256,128]{1,0:T(8,128)(2,1)S(1)}, bf16[256,128]{1,0:T(8,128)(2,1)}, u32[]{:S(2)}) copy-start(bf16[256,128]{1,0:T(8,128)(2,1)} %param.21) | copy-start | bytes 196612
  73.2 230.7 %all-gather.12.cloned.1.call-start = ((), (), s32[]{:S(2)}) async-start(), calls=%async_computation.3 | async-start | bytes 1179648 | tf_op jit(solution)/shard_map/all_gather | solution.py:185
  73.8 231.8 %all-gather.16.cloned.1.call-start = ((), (), s32[]{:S(2)}) async-start(), calls=%async_computation.5 | async-start | bytes 1179648 | tf_op jit(solution)/shard_map/all_gather | solution.py:186
  74.3 259.7 %reduce-scatter.2.cloned.1.call-start = ((), (), s32[]{:S(2)}) async-start(), calls=%async_computation.6 | async-start | bytes 1310720 | tf_op jit(solution)/shard_map/reduce_scatter | solution.py:188
  108.0 67.2 %copy-start.10 = (bf16[256,128]{1,0:T(8,128)(2,1)S(1)}, bf16[256,128]{1,0:T(8,128)(2,1)}, u32[]{:S(2)}) copy-start(bf16[256,128]{1,0:T(8,128)(2,1)} %param.20) | copy-start | bytes 196612
  140.8 67.7 %copy-start.16 = (f32[8]{0:T(128)S(1)}, f32[8]{0:T(128)}, u32[]{:S(2)}) copy-start(f32[8]{0:T(128)} %param.24) | copy-start | bytes 100
  140.8 67.8 %copy-start.15 = (f32[128]{0:T(128)S(1)}, f32[128]{0:T(128)}, u32[]{:S(2)}) copy-start(f32[128]{0:T(128)} %param.25) | copy-start | bytes 1540
  210.2 2.9 copy-start.2
  211.7 1.7 copy-start.3
  278.9 3.4 collective-permute-start
  280.4 1.9 copy-start.12
  280.4 1.9 copy-start.13
  280.5 1.9 copy-start.14
  280.5 1.9 copy-start.18
  280.5 1.9 copy-start.19
  284.7 3.5 %copy-start.5 = (bf16[2,1024,2,64]{1,3,2,0:T(8,128)(2,1)}, bf16[2,1024,2,64]{1,3,2,0:T(8,128)(2,1)S(1)}, u32[]{:S(2)}) copy-start(bf16[2,1024,2,64]{1,3,2,0:T(8,128)(2,1)S(1)} %get-tuple-element.339) | copy-start | bytes 1572868 | tf_op jit(solution)/shard_map/while
  289.0 2.4 copy-start.4
  289.0 2.4 copy-start.17
  293.1 1.0 copy-start.6
  294.1 3.4 %copy-start.5 = (bf16[2,1024,2,64]{1,3,2,0:T(8,128)(2,1)}, bf16[2,1024,2,64]{1,3,2,0:T(8,128)(2,1)S(1)}, u32[]{:S(2)}) copy-start(bf16[2,1024,2,64]{1,3,2,0:T(8,128)(2,1)S(1)} %get-tuple-element.339) | copy-start | bytes 1572868 | tf_op jit(solution)/shard_map/while
  298.4 2.4 copy-start.4
  298.4 2.4 copy-start.17
  302.4 1.0 copy-start.6
Sparse Core Ops, SparseCore 0:
  8.9 19.4 all-gather.17
  30.5 40.2 all-gather.7
  72.9 41.2 all-gather.13
  116.2 42.0 all-gather.9
  160.2 41.5 all-gather.11
  203.7 41.5 all-gather.15
  308.4 25.6 reduce-scatter.1
